TPU v7x, 32 devices: a whole 2x2x4 slice. The times are simulated.
32 devices in a mesh: ra: 4 (over y, x), cb: 8 (over z, core).
Axes of the slice: x: 2, y: 2, z: 4, core: 2. Of those that a mesh axis runs over, the one named last changes fastest.
Arguments:
- tokens: bfloat16 [512, 4096], P(None, 'ra'), may hold values from -40 to 40, as said below
- norm_gain: float32 [2, 4096], P(None, 'ra'), may hold values from 0.1 to 1.9
- gate_weight: bfloat16 [2, 4096, 11264], P(None, 'ra', 'cb'), may hold values from -0.09375 to 0.09375
- up_weight: bfloat16 [2, 4096, 11264], P(None, 'ra', 'cb'), may hold values from -0.09375 to 0.09375
- down_weight: bfloat16 [2, 11264, 4096], P(None, 'cb', 'ra'), may hold values from -0.0546875 to 0.0546875
Outputs:
- result: bfloat16 [512, 4096], P(None, 'ra')
Inputs may be any that keep to these rules, and one draw needn't show every extreme that they name: `tokens`: features come in blocks of 32 with scales that differ from block to block by up to a factor of 16.
All inputs are finite; a program needn't handle non-finite values.
Results may differ from a plain program's by a relative error of at most 0.0075.
Values may be sent and summed in bfloat16 or wider, within the bound.
A program may use at most 64 MiB of HBM per device.

v0:
```python
import jax
import jax.numpy as jnp
from jax import lax
from jax.sharding import PartitionSpec as P

D = 4096
LAYERS = 2


epsilon = 1e-06
keep_share = 0.5


def body(tokens, norm_gain, gate_weight, up_weight, down_weight):
    stream = tokens
    for layer in range(LAYERS):
        widened = stream.astype(jnp.float32)
        squares = jnp.sum(widened * widened, axis=1)
        normed = (widened * norm_gain[layer]).astype(jnp.bfloat16)
        gate_part = jnp.dot(normed, gate_weight[layer], preferred_element_type=jnp.float32)
        up_part = jnp.dot(normed, up_weight[layer], preferred_element_type=jnp.float32)
        total = lax.psum(squares, "ra")
        gate_share, up_share = (
            lax.psum_scatter(gate_part, "ra", scatter_dimension=1, tiled=True),
            lax.psum_scatter(up_part, "ra", scatter_dimension=1, tiled=True),
        )
        scale = lax.rsqrt(total / D + epsilon)[:, None]
        share = (jax.nn.silu(gate_share * scale) * (up_share * scale)).astype(jnp.bfloat16)
        hidden = lax.all_gather(share, "ra", axis=1, tiled=True)
        partial_down = jnp.dot(hidden, down_weight[layer], preferred_element_type=jnp.float32)
        branch = lax.psum(partial_down, "cb")
        stream = (keep_share * widened + branch).astype(jnp.bfloat16)
    return stream


def solution(mesh):
    placed = (
        P(None, "ra"),
        P(None, "ra"),
        P(None, "ra", "cb"),
        P(None, "ra", "cb"),
        P(None, "cb", "ra"),
    )
    return jax.shard_map(body, mesh=mesh, in_specs=placed, out_specs=P(None, "ra"), check_vma=False)
```

profile of v0, /device:TPU:1, one launch (start us, length us, event | category | flops | bytes accessed | tf_op | source)
XLA Modules:
  0.0 409.3 jit_solution(7383496427016766130)
XLA Ops:
  6.5 0.8 fusion.31
  7.3 5.4 %fusion.8 = f32[512,1408]{0,1:T(8,128)} fusion(bf16[2,1024,1408]{2,1,0:T(8,128)(2,1)} %param.8, bf16[512,1024]{1,0:T(8,128)(2,1)} %param.5, f32[1024]{0:T(1024)S(1)} %bitcast.24), kind=kOutput, calls=%fused_computation.14 | convolution fusion | flops 1477967872 | bytes 6819840 | tf_op jit(solution)/shard_map/dot_general | solution.py:21
  12.7 0.0 reduce-scatter.7.cloned.1.call-update
  12.8 0.0 reduce-scatter.5.cloned.1.call-start
  12.8 1.1 copy-done
  14.0 5.1 %fusion.10 = f32[512,1408]{0,1:T(8,128)} fusion(bf16[2,1024,1408]{2,1,0:T(8,128)(2,1)} %param.7, bf16[512,1024]{1,0:T(8,128)(2,1)S(1)} %copy-done, f32[1024]{0:T(1024)S(1)} %bitcast.25), kind=kOutput, calls=%fused_computation.16 | convolution fusion | flops 1477967872 | bytes 6819840 | tf_op jit(solution)/shard_map/dot_general | solution.py:20
  19.1 0.0 all-gather.3.cloned.1.call-start
  19.2 0.3 fusion.21
  19.5 9.3 %psum.28 = f32[512]{0:T(512)S(1)} all-reduce(f32[512]{0:T(512)S(1)} %fusion.21), channel_id=1, replica_groups=mesh['ra'=4,'cb'=8] {'ra'}, use_global_device_ids=true, to_apply=%region_2.0 | all-reduce | flops 512 | bytes 4096 | tf_op jit(solution)/shard_map/psum | solution.py:22
  28.8 28.0 %reduce-scatter.7.cloned.1.call-done = f32[512,352]{0,1:T(8,128)} async-done(((f32[512,1408]{0,1:T(8,128)}), f32[512,352]{0,1:T(8,128)}) %reduce-scatter.7.cloned.1.call-update) | async-done | bytes 720912 | tf_op jit(solution)/shard_map/reduce_scatter | solution.py:25
  56.8 44.8 %reduce-scatter.5.cloned.1.call-done = f32[512,352]{0,1:T(8,128)} async-done(((f32[512,1408]{0,1:T(8,128)}), f32[512,352]{0,1:T(8,128)}) %reduce-scatter.5.cloned.1.call-update) | async-done | bytes 720912 | tf_op jit(solution)/shard_map/reduce_scatter | solution.py:24
  101.6 2.3 multiply_convert_fusion.1
  103.9 0.0 all-reduce.3.cloned.1.call-start
  104.0 29.9 %all-gather.3.cloned.1.call-done = bf16[512,1408]{0,1:T(8,128)(2,1)} async-done(((bf16[512,352]{0,1:T(8,128)(2,1)}), bf16[512,1408]{0,1:T(8,128)(2,1)}) %all-gather.3.cloned.1.call-update) | async-done | bytes 1441808 | tf_op jit(solution)/shard_map/all_gather | solution.py:29
  133.8 5.4 %fusion.6 = f32[512,1024]{1,0:T(8,128)} fusion(bf16[512,1408]{0,1:T(8,128)(2,1)} %all-gather.3.cloned.1.call-done, bf16[2,1408,1024]{2,1,0:T(8,128)(2,1)} %param.9), kind=kOutput, calls=%fused_computation.12 | convolution fusion | flops 1476395008 | bytes 6422528 | tf_op jit(solution)/shard_map/dot_general | solution.py:30
  139.3 0.0 reduce-scatter.9.cloned.1.call-start
  139.3 63.9 %all-reduce.3.cloned.1.call-done = f32[512,1024]{1,0:T(8,128)} async-done(((f32[512,1024]{1,0:T(8,128)}), f32[512,1024]{1,0:T(8,128)}) %all-reduce.3.cloned.1.call-update) | async-done | bytes 2097168 | tf_op jit(solution)/shard_map/psum | solution.py:31
  203.2 2.0 fusion.25
  205.3 5.1 %fusion.4 = f32[512,1408]{0,1:T(8,128)} fusion(bf16[2,1024,1408]{2,1,0:T(8,128)(2,1)} %param.7, bf16[512,1024]{1,0:T(8,128)(2,1)S(1)} %get-tuple-element.6, f32[1024]{0:T(1024)S(1)} %bitcast.22), kind=kOutput, calls=%fused_computation.10 | convolution fusion | flops 1477967872 | bytes 6819840 | tf_op jit(solution)/shard_map/dot_general | solution.py:20
  210.3 0.0 reduce-scatter.9.cloned.1.call-update
  210.4 0.0 reduce-scatter.11.cloned.1.call-start
  210.4 5.1 %fusion.2 = f32[512,1408]{0,1:T(8,128)} fusion(bf16[2,1024,1408]{2,1,0:T(8,128)(2,1)} %param.8, bf16[512,1024]{1,0:T(8,128)(2,1)S(1)} %get-tuple-element.6, f32[1024]{0:T(1024)S(1)} %bitcast.23), kind=kOutput, calls=%fused_computation.8 | convolution fusion | flops 1477967872 | bytes 6819840 | tf_op jit(solution)/shard_map/dot_general | solution.py:21
  215.6 0.0 all-gather.5.cloned.1.call-start
  215.6 8.3 %psum.30 = f32[512]{0:T(512)S(1)} all-reduce(f32[512]{0:T(512)S(1)} %get-tuple-element.5), channel_id=1, replica_groups=mesh['ra'=4,'cb'=8] {'ra'}, use_global_device_ids=true, to_apply=%region_7.8 | all-reduce | flops 512 | bytes 4096 | tf_op jit(solution)/shard_map/psum | solution.py:22
  224.0 29.4 %reduce-scatter.9.cloned.1.call-done = f32[512,352]{0,1:T(8,128)} async-done(((f32[512,1408]{0,1:T(8,128)}), f32[512,352]{0,1:T(8,128)}) %reduce-scatter.9.cloned.1.call-update) | async-done | bytes 720912 | tf_op jit(solution)/shard_map/reduce_scatter | solution.py:24
  253.3 44.7 %reduce-scatter.11.cloned.1.call-done = f32[512,352]{0,1:T(8,128)} async-done(((f32[512,1408]{0,1:T(8,128)}), f32[512,352]{0,1:T(8,128)}) %reduce-scatter.11.cloned.1.call-update) | async-done | bytes 720912 | tf_op jit(solution)/shard_map/reduce_scatter | solution.py:25
  298.0 2.3 multiply_convert_fusion
  300.3 0.0 all-reduce.5.cloned.1.call-start
  300.3 29.9 %all-gather.5.cloned.1.call-done = bf16[512,1408]{0,1:T(8,128)(2,1)} async-done(((bf16[512,352]{0,1:T(8,128)(2,1)}), bf16[512,1408]{0,1:T(8,128)(2,1)}) %all-gather.5.cloned.1.call-update) | async-done | bytes 1441808 | tf_op jit(solution)/shard_map/all_gather | solution.py:29
  330.2 5.4 %fusion = f32[512,1024]{1,0:T(8,128)} fusion(bf16[512,1408]{0,1:T(8,128)(2,1)} %all-gather.5.cloned.1.call-done, bf16[2,1408,1024]{2,1,0:T(8,128)(2,1)} %param.9), kind=kOutput, calls=%fused_computation.6 | convolution fusion | flops 1476395008 | bytes 6422528 | tf_op jit(solution)/shard_map/dot_general | solution.py:30
  335.6 63.9 %all-reduce.5.cloned.1.call-done = f32[512,1024]{1,0:T(8,128)} async-done(((f32[512,1024]{1,0:T(8,128)}), f32[512,1024]{1,0:T(8,128)}) %all-reduce.5.cloned.1.call-update) | async-done | bytes 2097168 | tf_op jit(solution)/shard_map/psum | solution.py:31
  399.6 2.9 fusion.23
  (10 shorter events, 0.1 us)
Async XLA Ops:
  6.5 50.3 %reduce-scatter.7.cloned.1.call-start = ((), (), s32[]{:S(2)}) async-start(), calls=%async_computation.5 | async-start | bytes 3604480 | tf_op jit(solution)/shard_map/reduce_scatter | solution.py:25
  12.7 1.2 copy-start
  12.8 88.8 %reduce-scatter.5.cloned.1.call-start = ((), (), s32[]{:S(2)}) async-start(), calls=%async_computation.4 | async-start | bytes 3604480 | tf_op jit(solution)/shard_map/reduce_scatter | solution.py:24
  19.1 114.7 %all-gather.3.cloned.1.call-start = ((), (), s32[]{:S(2)}) async-start(), calls=%async_computation.6 | async-start | bytes 1802240 | tf_op jit(solution)/shard_map/all_gather | solution.py:29
  103.9 99.3 %all-reduce.3.cloned.1.call-start = ((), (), s32[]{:S(2)}) async-start(), calls=%async_computation.7 | async-start | bytes 4194304 | tf_op jit(solution)/shard_map/psum | solution.py:31
  139.3 114.1 %reduce-scatter.9.cloned.1.call-start = ((), (), s32[]{:S(2)}) async-start(), calls=%async_computation.8 | async-start | bytes 3604480 | tf_op jit(solution)/shard_map/reduce_scatter | solution.py:24
  210.4 87.6 %reduce-scatter.11.cloned.1.call-start = ((), (), s32[]{:S(2)}) async-start(), calls=%async_computation.9 | async-start | bytes 3604480 | tf_op jit(solution)/shard_map/reduce_scatter | solution.py:25
  215.6 114.6 %all-gather.5.cloned.1.call-start = ((), (), s32[]{:S(2)}) async-start(), calls=%async_computation.10 | async-start | bytes 1802240 | tf_op jit(solution)/shard_map/all_gather | solution.py:29
  300.3 99.3 %all-reduce.5.cloned.1.call-start = ((), (), s32[]{:S(2)}) async-start(), calls=%async_computation.11 | async-start | bytes 4194304 | tf_op jit(solution)/shard_map/psum | solution.py:31
Sparse Core Ops, SparseCore 0:
  12.9 43.8 reduce-scatter.6
  59.9 41.7 reduce-scatter.4
  104.0 29.7 all-gather.2
  139.4 63.8 all-reduce.2
  210.5 42.7 reduce-scatter.8
  256.2 41.7 reduce-scatter.10
  300.4 29.7 all-gather.4
  335.8 63.7 all-reduce.4
where the time goes:
time: 412 us; the launch traced here: 409 us
  waiting for transfers between devices  335 us (81%)
  matrix products  31.6 us (8%)
  blocking collectives  17.6 us (4%)
  between operations  13.5 us (3%)
  other arithmetic  9.81 us (2%)
    psum x2, waiting for transfers between devices, body(): branch = lax.psum(partial_down, 'cb')  128 us
    reduce_scatter x2, waiting for transfers between devices, body(): lax.psum_scatter(gate_part, 'ra', scatter_dimension=1, tiled=True)  74.2 us
    reduce_scatter x2, waiting for transfers between devices, body(): lax.psum_scatter(up_part, 'ra', scatter_dimension=1, tiled=True)  72.7 us
    all_gather x2, waiting for transfers between devices, body(): hidden = lax.all_gather(share, 'ra', axis=1, tiled=True)  59.7 us
    psum x2, blocking collectives, body(): total = lax.psum(squares, 'ra')  17.6 us
    dot_general x2, matrix products, body(): jnp.dot(hidden, down_weight[layer], preferred_element_type=jnp.float32)  10.8 us
    dot_general x2, matrix products, body(): jnp.dot(normed, up_weight[layer], preferred_element_type=jnp.float32)  10.6 us
    dot_general x2, matrix products, body(): jnp.dot(normed, gate_weight[layer], preferred_element_type=jnp.float32)  10.2 us
  transfers between devices with their start and end apart: 8, of which 8 were waited for; matrix products, arithmetic and copies ran while one was open for 3% of the time, Pallas kernels for 0%

commit v1 on v0

v1 whole, which is shorter than its diff:
```python
import functools
import math

import jax
import jax.numpy as jnp
from jax import lax
from jax.experimental import pallas as pl
from jax.experimental.pallas import tpu as pltpu
from jax.sharding import PartitionSpec as P

MESH = pl.DeviceIdType.MESH
EPSILON = 1e-06
KEEP_SHARE = 0.5
DEPTH = 4
F32 = jnp.float32
BF16 = jnp.bfloat16


def column_tiles(width, tile, visit):
    for start in range(0, width, tile):
        visit(start, min(tile, width - start))


def kernel(cfg, tok, gain, wg_hbm, up_hbm, wd_hbm, out,
           stream, wg, wu, wd, gbuf, ubuf, r1g, r1u, s1g, s1u, r2g, r2u, ssl, ssr,
           hid, pbuf, crecv, cs, zr, wsem, tsem, osem, ssem, rsem):
    nx, ny, nz, layers, chunks, features = (cfg[n] for n in ("nx", "ny", "nz", "layers", "chunks", "features"))
    nra = nx * ny
    period = max(chunks, DEPTH)
    r = lax.axis_index("ra")
    b = lax.axis_index("cb")
    x0, y0 = lax.rem(r, nx), lax.div(r, nx)
    core, z0 = lax.rem(b, 2), lax.div(b, 2)
    rw, ff = gbuf.shape[3], gbuf.shape[4]
    half = rw // 2
    tc = nra * rw
    dl = stream.shape[-1]
    rz = stream.shape[4]

    def load_w(layer, which):
        src, dst = ((wg_hbm, wg), (up_hbm, wu), (wd_hbm, wd))[which]
        return pltpu.make_async_copy(src.at[layer], dst.at[layer], wsem.at[layer, which])

    tokens_in = pltpu.make_async_copy(tok, stream.at[0], tsem.at[0])
    tokens_in.start()
    for layer in range(layers):
        for which in range(3):
            load_w(layer, which).start()

    barrier = pltpu.get_barrier_semaphore()
    for d in range(1, nra):
        pl.semaphore_signal(barrier, inc=1, device_id={"ra": lax.rem(r + d, nra)}, device_id_type=MESH)
    for d in range(1, nz):
        pl.semaphore_signal(barrier, inc=1, device_id={"cb": lax.rem(z0 + d, nz) * 2 + core}, device_id_type=MESH)
    pl.semaphore_signal(barrier, inc=1, device_id={"cb": z0 * 2 + 1 - core}, device_id_type=MESH)
    pl.semaphore_wait(barrier, nra + nz - 1)

    base = {}
    at = 0
    for name, count in cfg["kinds"]:
        base[name] = at
        at += count

    def remote(k, name, i, src, dst, device):
        return pltpu.make_async_remote_copy(
            src_ref=src, dst_ref=dst, send_sem=ssem.at[k, base[name] + i], recv_sem=rsem.at[k, base[name] + i],
            device_id=device, device_id_type=MESH)

    def to_x(d):
        xp = lax.rem(x0 + d, nx)
        return xp, {"ra": y0 * nx + xp}

    def to_y(d):
        yp = lax.rem(y0 + d, ny)
        return yp, {"ra": yp * nx + x0}

    def to_z(d):
        zp = lax.rem(z0 + d, nz)
        return zp, {"cb": zp * 2 + core}

    partner = {"cb": z0 * 2 + 1 - core}

    def copies(name, layer, c):
        k = layer * chunks + c
        made = []
        if name == "g1":
            for d in range(1, nx):
                xp, dev = to_x(d)
                made.append(remote(k, name, d - 1, gbuf.at[k, :, xp], r1g.at[k, d - 1], dev))
        if name == "u1":
            for d in range(1, ny):
                yp, dev = to_y(d)
                made.append(remote(k, name, d - 1, ubuf.at[k, yp], r1u.at[k, d - 1], dev))
        if name == "ss":
            for d in range(1, nra):
                made.append(remote(k, name, d - 1, ssl.at[k], ssr.at[k, d - 1], {"ra": lax.rem(r + d, nra)}))
        if name == "g2":
            for d in range(1, ny):
                yp, dev = to_y(d)
                made.append(remote(k, name, d - 1, s1g.at[k, yp], r2g.at[k, d - 1], dev))
        if name == "u2":
            for d in range(1, nx):
                xp, dev = to_x(d)
                made.append(remote(k, name, d - 1, s1u.at[k, xp], r2u.at[k, d - 1], dev))
        if name == "a1":
            for d in range(1, nx):
                part = hid.at[k, y0, x0, pl.ds(0, half)]
                made.append(remote(k, name, d - 1, part, part, to_x(d)[1]))
            for d in range(1, ny):
                part = hid.at[k, y0, x0, pl.ds(half, half)]
                made.append(remote(k, name, nx - 1 + d - 1, part, part, to_y(d)[1]))
        if name == "a2":
            for d in range(1, ny):
                part = hid.at[k, y0, :, pl.ds(0, half)]
                made.append(remote(k, name, d - 1, part, part, to_y(d)[1]))
            for d in range(1, nx):
                part = hid.at[k, :, x0, pl.ds(half, half)]
                made.append(remote(k, name, ny - 1 + d - 1, part, part, to_x(d)[1]))
        if name == "c1":
            made.append(remote(k, name, 0, pbuf.at[k, 1 - core], crecv.at[k], partner))
        if name == "z1":
            for d in range(1, nz):
                zp, dev = to_z(d)
                made.append(remote(k, name, d - 1, cs.at[k, zp], zr.at[k, d - 1], dev))
        if name == "z2":
            for d in range(1, nz):
                part = stream.at[layer + 1, c, core, z0]
                made.append(remote(k, name, d - 1, part, part, to_z(d)[1]))
        if name == "c2":
            part = stream.at[layer + 1, c, core]
            made.append(remote(k, name, 0, part, part, partner))
        return made

    def start(name, layer, c):
        for copy in copies(name, layer, c):
            copy.start()

    def arrived(name, layer, c):
        for copy in copies(name, layer, c):
            copy.wait_recv()

    def stage0(layer, c):
        k = layer * chunks + c

        @pl.when((layer == 0) & (c == 0))
        def _():
            tokens_in.wait()

        @pl.when(layer > 0)
        def _():
            arrived("c2", layer - 1, c)

        @pl.when(c == 0)
        def _():
            load_w(layer, 0).wait()
            load_w(layer, 1).wait()

        wide = stream[layer, c].reshape(tc, dl).astype(F32)
        normed = (wide * gain[layer]).astype(BF16)

        def gate_tile(s, w):
            part = jnp.dot(normed, wg[layer, :, s:s + w], preferred_element_type=F32)
            gbuf[k, :, :, :, s:s + w] = part.astype(BF16).reshape(ny, nx, rw, w)

        def up_tile(s, w):
            part = jnp.dot(normed, wu[layer, :, s:s + w], preferred_element_type=F32)
            ubuf[k, :, :, :, s:s + w] = part.astype(BF16).reshape(ny, nx, rw, w)

        column_tiles(ff, 512, gate_tile)
        start("g1", layer, c)
        column_tiles(ff, 512, up_tile)
        start("u1", layer, c)
        column = jnp.sum(wide * wide, axis=1, keepdims=True)
        diagonal = lax.broadcasted_iota(jnp.int32, (tc, tc), 0) == lax.broadcasted_iota(jnp.int32, (tc, tc), 1)
        ssl[k] = jnp.broadcast_to(jnp.sum(jnp.where(diagonal, column, 0.0), axis=0, keepdims=True), (8, tc))
        start("ss", layer, c)

    def stage1(layer, c):
        k = layer * chunks + c
        arrived("g1", layer, c)
        total = gbuf[k, :, x0].astype(F32)
        for d in range(nx - 1):
            total = total + r1g[k, d].astype(F32)
        s1g[k] = total.astype(BF16)
        start("g2", layer, c)
        arrived("u1", layer, c)
        total = ubuf[k, y0].astype(F32)
        for d in range(ny - 1):
            total = total + r1u[k, d].astype(F32)
        s1u[k] = total.astype(BF16)
        start("u2", layer, c)

    def stage2(layer, c):
        k = layer * chunks + c
        arrived("ss", layer, c)
        squares = ssl[k, 0:1]
        for d in range(nra - 1):
            squares = squares + ssr[k, d, 0:1]
        mine = lax.broadcasted_iota(jnp.int32, (rw, tc), 0) + r * rw == lax.broadcasted_iota(jnp.int32, (rw, tc), 1)
        column = jnp.sum(jnp.where(mine, squares, 0.0), axis=1, keepdims=True)
        scale = lax.rsqrt(column / features + EPSILON)
        arrived("g2", layer, c)
        arrived("u2", layer, c)
        gate = s1g[k, y0].astype(F32)
        for d in range(ny - 1):
            gate = gate + r2g[k, d].astype(F32)
        up = s1u[k, x0].astype(F32)
        for d in range(nx - 1):
            up = up + r2u[k, d].astype(F32)
        hid[k, y0, x0] = (jax.nn.silu(gate * scale) * (up * scale)).astype(BF16)
        start("a1", layer, c)

    def stage3(layer, c):
        arrived("a1", layer, c)
        start("a2", layer, c)

    def stage4(layer, c):
        k = layer * chunks + c
        arrived("a2", layer, c)

        @pl.when(c == 0)
        def _():
            load_w(layer, 2).wait()

        full = hid[k].reshape(tc, ff)

        def down_tile(s, w):
            part = jnp.dot(full, wd[layer, :, s:s + w], preferred_element_type=F32)
            pbuf[k, :, :, :, s:s + w] = part.astype(BF16).reshape(2, nz, rz, w)

        column_tiles(dl, 512, down_tile)
        start("c1", layer, c)

    def stage5(layer, c):
        k = layer * chunks + c
        arrived("c1", layer, c)
        cs[k] = (pbuf[k, core].astype(F32) + crecv[k].astype(F32)).astype(BF16)
        start("z1", layer, c)

    def stage6(layer, c):
        k = layer * chunks + c
        arrived("z1", layer, c)
        branch = cs[k, z0].astype(F32)
        for d in range(nz - 1):
            branch = branch + zr[k, d].astype(F32)
        kept = stream[layer, c, core, z0].astype(F32)
        stream[layer + 1, c, core, z0] = (KEEP_SHARE * kept + branch).astype(BF16)
        start("z2", layer, c)

    def stage7(layer, c):
        arrived("z2", layer, c)
        start("c2", layer, c)

    def write_out(c):
        return pltpu.make_async_copy(stream.at[layers, c], out.at[c], osem.at[c])

    def stage8(layer, c):
        @pl.when(layer == layers - 1)
        def _():
            arrived("c2", layer, c)
            write_out(c).start()

    def run(stage, u, offset):
        v = u - offset
        layer, c = lax.div(v, period), lax.rem(v, period)

        @pl.when((v >= 0) & (layer < layers) & (c < chunks))
        def _():
            stage(layer, c)

    def step(u, carry):
        for stage, offset in cfg["order"]:
            run((stage0, stage1, stage2, stage3, stage4, stage5, stage6, stage7, stage8)[stage], u, offset)
        return carry

    lax.fori_loop(0, layers * period + DEPTH, step, 0)

    def finish(k, carry):
        layer, c = lax.div(k, chunks), lax.rem(k, chunks)
        for name, _ in cfg["kinds"]:
            for copy in copies(name, layer, c):
                copy.wait_send()
        return carry

    lax.fori_loop(0, layers * chunks, finish, 0)
    for c in range(chunks):
        write_out(c).wait()


ORDER = ((0, 0), (2, 1), (4, 2), (6, 3), (8, 4), (1, 0), (3, 1), (5, 2), (7, 3))


def solution(mesh):
    nra, ncb = mesh.shape["ra"], mesh.shape["cb"]
    ny = max(d for d in range(1, math.isqrt(nra) + 1) if nra % d == 0)
    nx = nra // ny
    nz = ncb // 2

    def body(tokens, norm_gain, gate_weight, up_weight, down_weight):
        rows, dl = tokens.shape
        layers, _, ff = gate_weight.shape
        tc = min(rows, max(32 * nra, 16 * ncb))
        chunks = rows // tc
        rw, rz = tc // nra, tc // ncb
        items = layers * chunks
        kinds = (("g1", nx - 1), ("u1", ny - 1), ("ss", nra - 1), ("g2", ny - 1), ("u2", nx - 1),
                 ("a1", nx + ny - 2), ("a2", nx + ny - 2), ("c1", 1), ("z1", nz - 1), ("z2", nz - 1), ("c2", 1))
        sems = sum(n for _, n in kinds)
        cfg = dict(nx=nx, ny=ny, nz=nz, layers=layers, chunks=chunks, features=dl * nra, kinds=kinds, order=ORDER)
        hbm = pl.BlockSpec(memory_space=pl.ANY)
        vmem = pl.BlockSpec(memory_space=pltpu.VMEM)
        shaped = (chunks, 2, nz, rz, dl)
        result = pl.pallas_call(
            functools.partial(kernel, cfg),
            out_shape=jax.ShapeDtypeStruct(shaped, BF16),
            in_specs=[hbm, vmem, hbm, hbm, hbm],
            out_specs=hbm,
            scratch_shapes=[
                pltpu.VMEM((layers + 1,) + shaped, BF16),
                pltpu.VMEM((layers, dl, ff), BF16),
                pltpu.VMEM((layers, dl, ff), BF16),
                pltpu.VMEM((layers, ff, dl), BF16),
                pltpu.VMEM((items, ny, nx, rw, ff), BF16),
                pltpu.VMEM((items, ny, nx, rw, ff), BF16),
                pltpu.VMEM((items, nx - 1, ny, rw, ff), BF16),
                pltpu.VMEM((items, ny - 1, nx, rw, ff), BF16),
                pltpu.VMEM((items, ny, rw, ff), BF16),
                pltpu.VMEM((items, nx, rw, ff), BF16),
                pltpu.VMEM((items, ny - 1, rw, ff), BF16),
                pltpu.VMEM((items, nx - 1, rw, ff), BF16),
                pltpu.VMEM((items, 8, tc), F32),
                pltpu.VMEM((items, nra - 1, 8, tc), F32),
                pltpu.VMEM((items, ny, nx, rw, ff), BF16),
                pltpu.VMEM((items, 2, nz, rz, dl), BF16),
                pltpu.VMEM((items, nz, rz, dl), BF16),
                pltpu.VMEM((items, nz, rz, dl), BF16),
                pltpu.VMEM((items, nz - 1, rz, dl), BF16),
                pltpu.SemaphoreType.DMA((layers, 3)),
                pltpu.SemaphoreType.DMA((1,)),
                pltpu.SemaphoreType.DMA((chunks,)),
                pltpu.SemaphoreType.DMA((items, sems)),
                pltpu.SemaphoreType.DMA((items, sems)),
            ],
            compiler_params=pltpu.CompilerParams(
                collective_id=0, has_side_effects=True, vmem_limit_bytes=67_043_328),
            name="sublayers",
        )(tokens.reshape(shaped), norm_gain.reshape(layers, 1, dl), gate_weight, up_weight, down_weight)
        return result.reshape(rows, dl)

    placed = (
        P(None, "ra"),
        P(None, "ra"),
        P(None, "ra", "cb"),
        P(None, "ra", "cb"),
        P(None, "cb", "ra"),
    )
    return jax.shard_map(body, mesh=mesh, in_specs=placed, out_specs=P(None, "ra"), check_vma=False)
```

time: 412 us -> 115 us (0.28)
  waiting for transfers between devices: 335 us -> 0 us
  Pallas kernels: 0 us -> 111 us
  matrix products: 31.6 us -> 0 us
  blocking collectives: 17.6 us -> 0 us
  between operations: 13.5 us -> 0.01 us
  other arithmetic: 9.81 us -> 0 us
    reduce_scatter x4 -> x0, waiting for transfers between devices: 147 us -> none  [the longest x2 74.2 us: body(): lax.psum_scatter(gate_part, 'ra', scatter_dimension=1, tiled=True)]
    psum x2 -> x0, waiting for transfers between devices: 128 us -> none  [body(): branch = lax.psum(partial_down, 'cb')]
    pallas_call x0 -> x1, Pallas kernels: none -> 111 us  [body(): pl.pallas_call(functools.partial(kernel, cfg), out_shape=jax.ShapeDtypeSt...]
    all_gather x2 -> x0, waiting for transfers between devices: 59.7 us -> none  [body(): hidden = lax.all_gather(share, 'ra', axis=1, tiled=True)]
    dot_general x6 -> x0, matrix products: 31.6 us -> none  [the longest x2 10.8 us: body(): jnp.dot(hidden, down_weight[layer], preferred_element_type=jnp.float32)]
    psum x2 -> x0, blocking collectives: 17.6 us -> none  [body(): total = lax.psum(squares, 'ra')]
    convert_element_type x3 -> x0, other arithmetic: 7.47 us -> none  [the longest x2 4.55 us: body(): (jax.nn.silu(gate_share * scale) * (up_share * scale)).astype(jnp.bfloat16)]
  transfers between devices with their start and end apart: 8 -> 0, of which waited for: 8 -> 0; matrix products, arithmetic and copies ran while one was open for 3% -> 0% of each run, Pallas kernels for 0% -> 0%
where the time goes in v1:
time: 115 us
  Pallas kernels  111 us (97%)
  local copies, waits for them, and re-layouts  3.56 us (3%)
    pallas_call x1, Pallas kernels, body(): pl.pallas_call(functools.partial(kernel, cfg), out_shape=jax.ShapeDtypeSt...  111 us

profile of v1, /device:TPU:1, one launch (start us, length us, event | category | flops | bytes accessed | tf_op | source)
XLA Modules:
  0.0 114.6 jit_solution(15012560442168978778)
XLA Ops:
  0.0 1.3 %reshape.10.gain = f32[2,1,1024]{2,1,0:T(1,128)} reshape(f32[2,1024]{1,0:T(2,128)} %param.6) | data formatting | bytes 16384 | tf_op jit(solution)/shard_map/reshape | solution.py:347
  1.3 111.1 %sublayers.1 = bf16[4,2,4,16,1024]{4,3,2,1,0:T(8,128)(2,1)} custom-call(bf16[4,2,4,16,1024]{4,3,2,1,0:T(8,128)(2,1)} %bitcast.3, f32[2,1,1024]{2,1,0:T(1,128)} %reshape.10.gain, bf16[2,1024,1408]{2,1,0:T(8,128)(2,1)} %wg_hbm.1, bf16[2,1024,1408]{2,1,0:T(8,128)(2,1)} %up_hbm.1, bf16[2,1408,1024]{2,1,0:T(8,128)(2,1)} %wd_hbm.1), custom_call_target="tpu_custom_call" | custom-call | tf_op jit(solution)/shard_map/sublayers/pallas_call | solution.py:313
  112.4 2.3 %copy.7 = bf16[512,1024]{1,0:T(8,128)(2,1)} copy(bf16[512,1024]{1,0:T(8,128)(2,1)} %bitcast.2) | data formatting | bytes 2097152

commit v2 on v1

--- a/solution.py
+++ b/solution.py
@@ -23,7 +23,7 @@
 
 def kernel(cfg, tok, gain, wg_hbm, up_hbm, wd_hbm, out,
            stream, wg, wu, wd, gbuf, ubuf, r1g, r1u, s1g, s1u, r2g, r2u, ssl, ssr,
-           hid, pbuf, crecv, cs, zr, wsem, tsem, osem, ssem, rsem):
+           gown, uown, s1gown, s1uown, pown, csown, hid, pbuf, crecv, cs, zr, wsem, tsem, osem, ssem, rsem):
     nx, ny, nz, layers, chunks, features = (cfg[n] for n in ("nx", "ny", "nz", "layers", "chunks", "features"))
     nra = nx * ny
     period = max(chunks, DEPTH)
@@ -43,9 +43,8 @@
 
     tokens_in = pltpu.make_async_copy(tok, stream.at[0], tsem.at[0])
     tokens_in.start()
-    for layer in range(layers):
-        for which in range(3):
-            load_w(layer, which).start()
+    load_w(0, 0).start()
+    load_w(0, 1).start()
 
     barrier = pltpu.get_barrier_semaphore()
     for d in range(1, nra):
@@ -153,21 +152,36 @@
         @pl.when(c == 0)
         def _():
             load_w(layer, 0).wait()
-            load_w(layer, 1).wait()
 
         wide = stream[layer, c].reshape(tc, dl).astype(F32)
         normed = (wide * gain[layer]).astype(BF16)
 
         def gate_tile(s, w):
             part = jnp.dot(normed, wg[layer, :, s:s + w], preferred_element_type=F32)
-            gbuf[k, :, :, :, s:s + w] = part.astype(BF16).reshape(ny, nx, rw, w)
+            part = part.reshape(ny, nx, rw, w)
+            gown[:, :, :, s:s + w] = part
+            gbuf[k, :, :, :, s:s + w] = part.astype(BF16)
 
         def up_tile(s, w):
             part = jnp.dot(normed, wu[layer, :, s:s + w], preferred_element_type=F32)
-            ubuf[k, :, :, :, s:s + w] = part.astype(BF16).reshape(ny, nx, rw, w)
+            part = part.reshape(ny, nx, rw, w)
+            uown[:, :, :, s:s + w] = part
+            ubuf[k, :, :, :, s:s + w] = part.astype(BF16)
 
         column_tiles(ff, 512, gate_tile)
         start("g1", layer, c)
+
+        @pl.when(c == 0)
+        def _():
+            load_w(layer, 1).wait()
+
+        @pl.when((layer == 0) & (c == 0))
+        def _():
+            load_w(0, 2).start()
+            for later in range(1, layers):
+                for which in range(3):
+                    load_w(later, which).start()
+
         column_tiles(ff, 512, up_tile)
         start("u1", layer, c)
         column = jnp.sum(wide * wide, axis=1, keepdims=True)
@@ -178,16 +192,18 @@
     def stage1(layer, c):
         k = layer * chunks + c
         arrived("g1", layer, c)
-        total = gbuf[k, :, x0].astype(F32)
+        total = gown[:, x0]
         for d in range(nx - 1):
             total = total + r1g[k, d].astype(F32)
         s1g[k] = total.astype(BF16)
+        s1gown[k] = total
         start("g2", layer, c)
         arrived("u1", layer, c)
-        total = ubuf[k, y0].astype(F32)
+        total = uown[y0]
         for d in range(ny - 1):
             total = total + r1u[k, d].astype(F32)
         s1u[k] = total.astype(BF16)
+        s1uown[k] = total
         start("u2", layer, c)
 
     def stage2(layer, c):
@@ -201,10 +217,10 @@
         scale = lax.rsqrt(column / features + EPSILON)
         arrived("g2", layer, c)
         arrived("u2", layer, c)
-        gate = s1g[k, y0].astype(F32)
+        gate = s1gown[k, y0]
         for d in range(ny - 1):
             gate = gate + r2g[k, d].astype(F32)
-        up = s1u[k, x0].astype(F32)
+        up = s1uown[k, x0]
         for d in range(nx - 1):
             up = up + r2u[k, d].astype(F32)
         hid[k, y0, x0] = (jax.nn.silu(gate * scale) * (up * scale)).astype(BF16)
@@ -226,7 +242,9 @@
 
         def down_tile(s, w):
             part = jnp.dot(full, wd[layer, :, s:s + w], preferred_element_type=F32)
-            pbuf[k, :, :, :, s:s + w] = part.astype(BF16).reshape(2, nz, rz, w)
+            part = part.reshape(2, nz, rz, w)
+            pown[:, :, :, s:s + w] = part
+            pbuf[k, :, :, :, s:s + w] = part.astype(BF16)
 
         column_tiles(dl, 512, down_tile)
         start("c1", layer, c)
@@ -234,13 +252,15 @@
     def stage5(layer, c):
         k = layer * chunks + c
         arrived("c1", layer, c)
-        cs[k] = (pbuf[k, core].astype(F32) + crecv[k].astype(F32)).astype(BF16)
+        total = pown[core] + crecv[k].astype(F32)
+        csown[k] = total
+        cs[k] = total.astype(BF16)
         start("z1", layer, c)
 
     def stage6(layer, c):
         k = layer * chunks + c
         arrived("z1", layer, c)
-        branch = cs[k, z0].astype(F32)
+        branch = csown[k, z0]
         for d in range(nz - 1):
             branch = branch + zr[k, d].astype(F32)
         kept = stream[layer, c, core, z0].astype(F32)
@@ -287,7 +307,7 @@
         write_out(c).wait()
 
 
-ORDER = ((0, 0), (2, 1), (4, 2), (6, 3), (8, 4), (1, 0), (3, 1), (5, 2), (7, 3))
+ORDER = ((8, 4), (0, 0), (6, 3), (4, 2), (2, 1), (5, 2), (3, 1), (7, 3), (1, 0))
 
 
 def solution(mesh):
@@ -330,6 +350,12 @@
                 pltpu.VMEM((items, nx - 1, rw, ff), BF16),
                 pltpu.VMEM((items, 8, tc), F32),
                 pltpu.VMEM((items, nra - 1, 8, tc), F32),
+                pltpu.VMEM((ny, nx, rw, ff), F32),
+                pltpu.VMEM((ny, nx, rw, ff), F32),
+                pltpu.VMEM((items, ny, rw, ff), F32),
+                pltpu.VMEM((items, nx, rw, ff), F32),
+                pltpu.VMEM((2, nz, rz, dl), F32),
+                pltpu.VMEM((items, nz, rz, dl), F32),
                 pltpu.VMEM((items, ny, nx, rw, ff), BF16),
                 pltpu.VMEM((items, 2, nz, rz, dl), BF16),
                 pltpu.VMEM((items, nz, rz, dl), BF16),

time: 115 us -> 112 us (0.974)
  Pallas kernels: 111 us -> 108 us
    pallas_call x1, Pallas kernels: 111 us -> 108 us  [body(): pl.pallas_call(functools.partial(kernel, cfg), out_shape=jax.ShapeDtypeSt...]
where the time goes in v2:
time: 112 us; the launch traced here: 111 us
  Pallas kernels  108 us (96%)
  local copies, waits for them, and re-layouts  3.56 us (3%)
    pallas_call x1, Pallas kernels, body(): pl.pallas_call(functools.partial(kernel, cfg), out_shape=jax.ShapeDtypeSt...  108 us
    unnamed x1, local copies, waits for them, and re-layouts  2.26 us

profile of v2, /device:TPU:1, one launch (start us, length us, event | category | flops | bytes accessed | tf_op | source)
XLA Modules:
  0.0 111.4 jit_solution(7344532724359167448)
XLA Ops:
  0.0 1.3 %reshape.10.gain = f32[2,1,1024]{2,1,0:T(1,128)} reshape(f32[2,1024]{1,0:T(2,128)} %param.6) | data formatting | bytes 16384 | tf_op jit(solution)/shard_map/reshape | solution.py:373
  1.3 107.8 %sublayers.1 = bf16[4,2,4,16,1024]{4,3,2,1,0:T(8,128)(2,1)} custom-call(bf16[4,2,4,16,1024]{4,3,2,1,0:T(8,128)(2,1)} %bitcast.3, f32[2,1,1024]{2,1,0:T(1,128)} %reshape.10.gain, bf16[2,1024,1408]{2,1,0:T(8,128)(2,1)} %wg_hbm.1, bf16[2,1024,1408]{2,1,0:T(8,128)(2,1)} %up_hbm.1, bf16[2,1408,1024]{2,1,0:T(8,128)(2,1)} %wd_hbm.1), custom_call_target="tpu_custom_call" | custom-call | tf_op jit(solution)/shard_map/sublayers/pallas_call | solution.py:333
  109.1 2.3 %copy.7 = bf16[512,1024]{1,0:T(8,128)(2,1)} copy(bf16[512,1024]{1,0:T(8,128)(2,1)} %bitcast.2) | data formatting | bytes 2097152
